TPU v7x, 32 devices: a whole 2x2x4 slice. The times are simulated.
32 devices in a mesh: kv: 8 (over z, x), tp: 4 (over y, core).
Axes of the slice: x: 2, y: 2, z: 4, core: 2. Of those that a mesh axis runs over, the one named last changes fastest.
Arguments:
- inputs: bfloat16 [2048, 2048], P('kv', 'tp'), may hold values from -6 to 6
- queries: bfloat16 [2048, 2048], P('kv', 'tp'), may hold values from -8 to 8
- key_vectors: bfloat16 [2048, 512], P('kv', 'tp'), may hold values from -8 to 8
- value_rows_by_head: bfloat16 [2048, 512], P('kv', 'tp'), may hold values from -6 to 6
- out_grad: bfloat16 [2048, 2048], P('kv', 'tp'), may hold values from -6 to 6
- chosen: int32 [16, 16], replicated, may hold values from 0 to 31, as said below
Outputs:
- query_grad: bfloat16 [2048, 2048], P('kv', 'tp')
- key_grad: bfloat16 [2048, 512], P('kv', 'tp')
- value_grad: bfloat16 [2048, 512], P('kv', 'tp')
- weight_grad: float32 [2048, 2048], P('kv', 'tp')
Inputs may be any that keep to these rules, and one draw needn't show every extreme that they name: `chosen`: row r holds 16 distinct key-block numbers, among them every key block that intersects query block r. The rows of one device (aligned runs of 2 rows) name at most 2 distinct key blocks that lie on any one other device (aligned runs of 4 key blocks), and exactly 2 at some other device for some devices.
All inputs are finite; a program needn't handle non-finite values.
Results may differ from a plain program's by a relative error of at most 0.015.
The roundings to bfloat16 on the way count: a program that leaves them out, or rounds other values in their place, can miss the bound.
Values may be sent and summed in bfloat16 or wider, within the bound.
A program may use at most 128 MiB of HBM per device.

v0:
```python
import jax
import jax.numpy as jnp
from jax import lax
from jax.sharding import PartitionSpec as P

HEAD_SIZE = 64
QB = 128
KB = 64


def body(inputs, queries, key_vectors, value_rows_by_head, out_grad, chosen):
    score_scale = HEAD_SIZE ** (-0.5)
    rows_dev = queries.shape[0]
    q_heads = queries.shape[1] // HEAD_SIZE
    kv_heads = key_vectors.shape[1] // HEAD_SIZE
    group_size = q_heads // kv_heads
    local_blocks = rows_dev // QB
    device_index = lax.axis_index("kv")
    first_block = device_index * local_blocks
    whole_inputs = lax.all_gather(inputs, "tp", axis=1, tiled=True)
    all_keys, all_values = (
        lax.all_gather(key_vectors, "kv", axis=0, tiled=True),
        lax.all_gather(value_rows_by_head, "kv", axis=0, tiled=True),
    )
    offsets = jnp.arange(KB, dtype=jnp.int32)

    def attend_block(block_idx):
        q_blk = first_block + block_idx
        first = block_idx * QB
        q_block = lax.dynamic_slice_in_dim(queries, first, QB, 0).reshape(
            QB, kv_heads, group_size, HEAD_SIZE
        )
        g_block = lax.dynamic_slice_in_dim(out_grad, first, QB, 0).reshape(
            QB, kv_heads, group_size, HEAD_SIZE
        )
        key_rows = (chosen[q_blk][:, None] * KB + offsets[None, :]).reshape(-1)
        key_sel = jnp.take(all_keys, key_rows, axis=0).reshape(-1, kv_heads, HEAD_SIZE)
        val_sel = jnp.take(all_values, key_rows, axis=0).reshape(-1, kv_heads, HEAD_SIZE)
        positions = q_blk * QB + jnp.arange(QB, dtype=jnp.int32)
        allowed = key_rows[None, :] <= positions[:, None]
        scores = (
            jnp.einsum("tkgd,skd->kgts", q_block, key_sel, preferred_element_type=jnp.float32)
            * score_scale
        )
        scores = jnp.where(allowed, scores, -1e30)
        row_max = jnp.max(scores, axis=-1, keepdims=True)
        log_sum = row_max + jnp.log(jnp.sum(jnp.exp(scores - row_max), axis=-1, keepdims=True))
        probs = jnp.exp(scores - log_sum)
        probs_half = probs.astype(jnp.bfloat16)
        attended = jnp.einsum(
            "kgts,skd->tkgd", probs_half, val_sel, preferred_element_type=jnp.float32
        )
        row_dot = jnp.einsum("tkgd,tkgd->kgt", g_block.astype(jnp.float32), attended)
        prob_grad = jnp.einsum(
            "tkgd,skd->kgts", g_block, val_sel, preferred_element_type=jnp.float32
        )
        score_grad = (probs * (prob_grad - row_dot[..., None])).astype(jnp.bfloat16)
        d_query = (
            jnp.einsum("kgts,skd->tkgd", score_grad, key_sel, preferred_element_type=jnp.float32)
            * score_scale
        )
        d_key = (
            jnp.einsum("kgts,tkgd->skd", score_grad, q_block, preferred_element_type=jnp.float32)
            * score_scale
        )
        d_value = jnp.einsum(
            "kgts,tkgd->skd", probs_half, g_block, preferred_element_type=jnp.float32
        )
        return (
            d_query.reshape(QB, q_heads * HEAD_SIZE),
            key_rows,
            d_key.reshape(-1, kv_heads * HEAD_SIZE),
            d_value.reshape(-1, kv_heads * HEAD_SIZE),
        )

    def summed_step(state_pair, block_idx):
        acc_k, acc_v = state_pair
        d_query, key_rows, d_key, d_value = attend_block(block_idx)
        return ((acc_k.at[key_rows].add(d_key), acc_v.at[key_rows].add(d_value)), d_query)

    block_range = jnp.arange(local_blocks, dtype=jnp.int32)
    zeros = jnp.zeros((all_keys.shape[0], kv_heads * HEAD_SIZE), jnp.float32)
    (acc_k, acc_v), query_blocks = lax.scan(summed_step, (zeros, zeros), block_range)
    query_grad = query_blocks.reshape(rows_dev, q_heads * HEAD_SIZE).astype(jnp.bfloat16)
    n_dev = lax.axis_size("kv")
    owner_blocks = rows_dev // KB
    width = acc_k.shape[1]
    local_chosen = lax.dynamic_slice_in_dim(chosen, first_block, local_blocks, 0).reshape(-1)
    block_ids = jnp.arange(n_dev * owner_blocks, dtype=jnp.int32)
    used = jnp.any(local_chosen[:, None] == block_ids[None, :], axis=0).reshape(n_dev, owner_blocks)
    ranking = (
        used.astype(jnp.int32) * owner_blocks
        + (owner_blocks - 1 - jnp.arange(owner_blocks, dtype=jnp.int32))[None, :]
    )
    _, picks = lax.top_k(ranking, local_blocks)
    blocks_k = acc_k.reshape(n_dev, owner_blocks, KB, width)
    blocks_v = acc_v.reshape(n_dev, owner_blocks, KB, width)
    others = (jnp.arange(n_dev, dtype=jnp.int32) != device_index)[:, None, None, None]
    send_k = jnp.where(others, jnp.take_along_axis(blocks_k, picks[:, :, None, None], axis=1), 0.0)
    send_v = jnp.where(others, jnp.take_along_axis(blocks_v, picks[:, :, None, None], axis=1), 0.0)
    recv_k, recv_v, recv_ids = (
        lax.all_to_all(send_k, "kv", split_axis=0, concat_axis=0, tiled=True),
        lax.all_to_all(send_v, "kv", split_axis=0, concat_axis=0, tiled=True),
        lax.all_to_all(picks, "kv", split_axis=0, concat_axis=0, tiled=True),
    )
    one_hot = (
        recv_ids.reshape(-1)[:, None] == jnp.arange(owner_blocks, dtype=jnp.int32)[None, :]
    ).astype(jnp.float32)
    flat_k = recv_k.reshape(n_dev * local_blocks, KB * width)
    flat_v = recv_v.reshape(n_dev * local_blocks, KB * width)
    added_k = jnp.einsum("nb,nr->br", one_hot, flat_k, precision=lax.Precision.HIGHEST)
    added_v = jnp.einsum("nb,nr->br", one_hot, flat_v, precision=lax.Precision.HIGHEST)
    own_k = lax.dynamic_slice_in_dim(acc_k, device_index * rows_dev, rows_dev, 0)
    own_v = lax.dynamic_slice_in_dim(acc_v, device_index * rows_dev, rows_dev, 0)
    key_total = own_k + added_k.reshape(rows_dev, width)
    value_total = own_v + added_v.reshape(rows_dev, width)
    weight_grad = lax.psum_scatter(
        jnp.einsum(
            "tr,tc->rc", whole_inputs, query_grad, preferred_element_type=jnp.float32
        ).astype(jnp.bfloat16),
        "kv",
        scatter_dimension=0,
        tiled=True,
    ).astype(jnp.float32)
    return (
        query_grad,
        key_total.astype(jnp.bfloat16),
        value_total.astype(jnp.bfloat16),
        weight_grad,
    )


def solution(mesh):
    placed = (P("kv", "tp"), P("kv", "tp"), P("kv", "tp"), P("kv", "tp"), P("kv", "tp"), P())
    return jax.shard_map(
        body,
        mesh=mesh,
        in_specs=placed,
        out_specs=(P("kv", "tp"), P("kv", "tp"), P("kv", "tp"), P("kv", "tp")),
        check_vma=False,
    )
```

profile of v0, /device:TPU:0, one launch (start us, length us, event | category | flops | bytes accessed | tf_op | source)
XLA Modules:
  0.0 283.4 jit_solution(11448416967880059504)
XLA Ops:
  7.2 0.7 all-gather.2.cloned.1.call-update
  8.0 33.3 %all_gather.10 = bf16[2048,128]{1,0:T(8,128)(2,1)S(1)} all-gather(bf16[256,128]{1,0:T(8,128)(2,1)} %param.15), channel_id=1, replica_groups=mesh['kv'=8,'tp'=4] {'kv'}, dimensions={0}, use_global_device_ids=true | all-gather | bytes 589824 | tf_op jit(solution)/shard_map/all_gather | solution.py:23
  41.2 31.4 %all_gather.9 = bf16[2048,128]{1,0:T(8,128)(2,1)S(1)} all-gather(bf16[256,128]{1,0:T(8,128)(2,1)} %param.14), channel_id=1, replica_groups=mesh['kv'=8,'tp'=4] {'kv'}, dimensions={0}, use_global_device_ids=true | all-gather | bytes 589824 | tf_op jit(solution)/shard_map/all_gather | solution.py:22
  73.3 116.2 %while.15 = (s32[]{:T(128)}, f32[2048,128]{1,0:T(8,128)S(1)}, f32[2048,128]{1,0:T(8,128)S(1)}, bf16[2,128,512]{1,2,0:T(8,128)(2,1)}, s32[2]{0:T(128)}, /*index=5...) while((s32[]{:T(128)}, f32[2048,128]{1,0:T(8,128)S(1)}, ...), condition=%wide.region_5.7_spmd.clone, body=%wide.region_0.6_spmd.clone.sunk | while | flops 828452992 | bytes 84783232 | solution.py:83
  73.3 1.3 dynamic_slice.44
  75.2 0.7 fusion.68
  76.0 3.2 %gather_fusion = bf16[1024,128]{1,0:T(8,128)(2,1)S(1)} fusion(bf16[2048,128]{1,0:T(8,128)(2,1)S(1)} %get-tuple-element.313, s32[1024]{0:T(1024)S(1)} %fusion.69), kind=kCustom, calls=%fused_computation.2.clone.clone.1 | custom fusion | bytes 528384 | tf_op jit(solution)/shard_map/while/body/eval_jaxpr/jit(_take)/gather | solution.py:38
  79.3 4.3 %gather_fusion.1 = bf16[1024,128]{1,0:T(8,128)(2,1)} fusion(bf16[2048,128]{1,0:T(8,128)(2,1)S(1)} %get-tuple-element.312, s32[1024]{0:T(1024)S(1)} %fusion.69), kind=kCustom, calls=%fused_computation.clone.clone.1 | custom fusion | bytes 528384 | tf_op jit(solution)/shard_map/while/body/eval_jaxpr/jit(_take)/gather | solution.py:37
  83.6 1.9 broadcast_select_fusion.4
  85.5 1.1 copy.114
  87.5 1.7 constant_dynamic-slice_fusion.5
  89.1 1.7 copy.113
  90.8 1.7 fusion.70
  92.5 1.9 copy-done
  94.4 0.9 exponential_reduce_fusion.2
  95.3 1.7 copy.116
  96.9 4.1 %fusion.74 = f32[2,64,1024,1]{2,1,3,0:T(8,128)} fusion(bf16[128,2,4,64]{0,3,2,1:T(8,128)(2,1)} %bitcast.184, f32[2,1024,128,4]{2,1,3,0:T(8,128)} %copy-done, f32[2,4,128]{2,1,0:T(4,128)S(1)} %bitcast.197, pred[128,1024]{0,1:T(8,128)(4,1)S(1)} %broadcast_compare_fusion.2), kind=kOutput, calls=%fused_computation.37.clone.1 | convolution fusion | flops 138412032 | bytes 4984832 | tf_op jit(solution)/shard_map/while/body/eval_jaxpr/kgts,tkgd->skd/dot_general | solution.py:66
  101.1 2.0 copy.118
  103.2 6.8 %scatter_fusion.1 = f32[2048,128]{1,0:T(8,128)S(1)} fusion(f32[2048,128]{1,0:T(8,128)S(1)} %get-tuple-element.290, s32[1024]{0:T(1024)S(1)} %bitcast.193, f32[1024,128]{1,0:T(8,128)} %copy.118), kind=kCustom, calls=%fused_computation.5.clone.clone.1 | custom fusion | flops 131072 | bytes 1576960 | tf_op jit(solution)/shard_map/while/body/eval_jaxpr/scatter-add | solution.py:79
  110.1 1.8 copy.115
  111.9 3.4 %fusion.71 = f32[2,4,128]{2,1,0:T(4,128)S(1)} fusion(bf16[1024,2,64,1]{0,2,3,1:T(8,128)(2,1)} %bitcast.182, bf16[2,4,128,64]{2,3,1,0:T(8,128)(2,1)} %bitcast.185, f32[2,1024,128,4]{2,1,3,0:T(8,128)} %copy-done, f32[2,4,128]{2,1,0:T(4,128)S(1)} %bitcast.198, pred[128,1024]{0,1:T(8,128)(4,1)S(1)} %broadcast_compare_fusion.2), kind=kOutput, calls=%fused_computation.20.clone.1 | convolution fusion | flops 138607616 | bytes 4726784 | tf_op jit(solution)/shard_map/while/body/eval_jaxpr/kgts,skd->tkgd/dot_general | solution.py:50
  115.5 1.4 fusion.72
  116.9 1.3 copy-done.2
  118.2 1.5 fusion.73
  119.8 2.0 copy.117
  121.8 6.8 %scatter_fusion = f32[2048,128]{1,0:T(8,128)S(1)} fusion(f32[2048,128]{1,0:T(8,128)S(1)} %get-tuple-element.289, s32[1024]{0:T(1024)S(1)} %bitcast.194, f32[1024,128]{1,0:T(8,128)} %copy.117), kind=kCustom, calls=%fused_computation.4.clone.clone.1 | custom fusion | flops 131072 | bytes 1576960 | tf_op jit(solution)/shard_map/while/body/eval_jaxpr/scatter-add | solution.py:79
  128.6 2.1 convolution_multiply_fusion.2
  131.4 1.2 dynamic_slice.44
  133.3 0.7 fusion.68
  134.1 3.2 %gather_fusion = bf16[1024,128]{1,0:T(8,128)(2,1)S(1)} fusion(bf16[2048,128]{1,0:T(8,128)(2,1)S(1)} %get-tuple-element.313, s32[1024]{0:T(1024)S(1)} %fusion.69), kind=kCustom, calls=%fused_computation.2.clone.clone.1 | custom fusion | bytes 528384 | tf_op jit(solution)/shard_map/while/body/eval_jaxpr/jit(_take)/gather | solution.py:38
  137.3 4.3 %gather_fusion.1 = bf16[1024,128]{1,0:T(8,128)(2,1)} fusion(bf16[2048,128]{1,0:T(8,128)(2,1)S(1)} %get-tuple-element.312, s32[1024]{0:T(1024)S(1)} %fusion.69), kind=kCustom, calls=%fused_computation.clone.clone.1 | custom fusion | bytes 528384 | tf_op jit(solution)/shard_map/while/body/eval_jaxpr/jit(_take)/gather | solution.py:37
  141.6 1.9 broadcast_select_fusion.4
  143.6 1.1 copy.114
  145.5 1.7 constant_dynamic-slice_fusion.5
  147.2 1.7 copy.113
  148.9 1.7 fusion.70
  150.6 1.9 copy-done
  152.5 0.9 exponential_reduce_fusion.2
  153.3 1.7 copy.116
  155.0 4.1 %fusion.74 = f32[2,64,1024,1]{2,1,3,0:T(8,128)} fusion(bf16[128,2,4,64]{0,3,2,1:T(8,128)(2,1)} %bitcast.184, f32[2,1024,128,4]{2,1,3,0:T(8,128)} %copy-done, f32[2,4,128]{2,1,0:T(4,128)S(1)} %bitcast.197, pred[128,1024]{0,1:T(8,128)(4,1)S(1)} %broadcast_compare_fusion.2), kind=kOutput, calls=%fused_computation.37.clone.1 | convolution fusion | flops 138412032 | bytes 4984832 | tf_op jit(solution)/shard_map/while/body/eval_jaxpr/kgts,tkgd->skd/dot_general | solution.py:66
  159.2 2.0 copy.118
  161.3 6.8 %scatter_fusion.1 = f32[2048,128]{1,0:T(8,128)S(1)} fusion(f32[2048,128]{1,0:T(8,128)S(1)} %get-tuple-element.290, s32[1024]{0:T(1024)S(1)} %bitcast.193, f32[1024,128]{1,0:T(8,128)} %copy.118), kind=kCustom, calls=%fused_computation.5.clone.clone.1 | custom fusion | flops 131072 | bytes 1576960 | tf_op jit(solution)/shard_map/while/body/eval_jaxpr/scatter-add | solution.py:79
  168.1 1.8 copy.115
  169.9 3.4 %fusion.71 = f32[2,4,128]{2,1,0:T(4,128)S(1)} fusion(bf16[1024,2,64,1]{0,2,3,1:T(8,128)(2,1)} %bitcast.182, bf16[2,4,128,64]{2,3,1,0:T(8,128)(2,1)} %bitcast.185, f32[2,1024,128,4]{2,1,3,0:T(8,128)} %copy-done, f32[2,4,128]{2,1,0:T(4,128)S(1)} %bitcast.198, pred[128,1024]{0,1:T(8,128)(4,1)S(1)} %broadcast_compare_fusion.2), kind=kOutput, calls=%fused_computation.20.clone.1 | convolution fusion | flops 138607616 | bytes 4726784 | tf_op jit(solution)/shard_map/while/body/eval_jaxpr/kgts,skd->tkgd/dot_general | solution.py:50
  173.5 1.4 fusion.72
  174.9 1.3 copy-done.2
  176.3 1.5 fusion.73
  177.8 2.0 copy.117
  179.9 6.8 %scatter_fusion = f32[2048,128]{1,0:T(8,128)S(1)} fusion(f32[2048,128]{1,0:T(8,128)S(1)} %get-tuple-element.289, s32[1024]{0:T(1024)S(1)} %bitcast.194, f32[1024,128]{1,0:T(8,128)} %copy.117), kind=kCustom, calls=%fused_computation.4.clone.clone.1 | custom fusion | flops 131072 | bytes 1576960 | tf_op jit(solution)/shard_map/while/body/eval_jaxpr/scatter-add | solution.py:79
  186.7 2.1 convolution_multiply_fusion.2
  189.4 1.1 copy.72
  190.6 3.4 %fusion.15 = bf16[2048,512]{0,1:T(8,128)(2,1)} fusion(bf16[256,512]{1,0:T(8,128)(2,1)S(1)} %bitcast.191, bf16[256,2048]{1,0:T(8,128)(2,1)} %all-gather.2.cloned.1.call-done), kind=kOutput, calls=%fused_computation.39 | convolution fusion | flops 537919488 | bytes 3407872 | tf_op jit(solution)/shard_map/tr,tc->rc/dot_general | solution.py:118
  194.0 0.7 constant_dynamic-slice_fusion.3
  195.7 0.7 copy.74
  196.4 5.8 %all-to-all-start = ((s32[8,1,2]{2,1,0:T(1,128)}), s32[8,1,2]{2,1,0:T(1,128)S(1)}, u32[]{:S(2)}, u32[]{:S(2)}) async-start(s32[8,1,2]{2,1,0:T(1,128)} %copy.74), calls=%async_computation | async-start | bytes 8192 | tf_op jit(solution)/shard_map/all_to_all | solution.py:104
  203.1 1.4 gather_fusion.2
  204.6 2.0 select_select_fusion
  206.6 2.1 all-to-all-done
  208.7 26.8 %all_to_all.19 = f32[8,2,64,128]{3,2,1,0:T(8,128)S(1)} all-to-all(f32[8,2,64,128]{3,2,1,0:T(8,128)S(1)} %get-tuple-element.190), channel_id=1, replica_groups=mesh['kv'=8,'tp'=4] {'kv'}, dimensions={0} | all-to-all | bytes 1048576 | tf_op jit(solution)/shard_map/all_to_all | solution.py:102
  235.6 5.3 %all-to-all-start.2 = ((f32[8,2,64,128]{3,2,1,0:T(8,128)}), f32[8,2,64,128]{3,2,1,0:T(8,128)S(1)}, u32[]{:S(2)}, u32[]{:S(2)}) async-start(f32[8,2,64,128]{3,2,1,0:T(8,128)} %get-tuple-element.189), calls=%async_computation.2 | async-start | bytes 1048576 | tf_op jit(solution)/shard_map/all_to_all | solution.py:103
  242.9 8.3 %all-to-all-done.2 = f32[8,2,64,128]{3,2,1,0:T(8,128)S(1)} async-done(((f32[8,2,64,128]{3,2,1,0:T(8,128)}), f32[8,2,64,128]{3,2,1,0:T(8,128)S(1)}, u32[]{:S(2)}, u32[]{:S(2)}) %all-to-all-start.2) | async-done | bytes 524320 | tf_op jit(solution)/shard_map/all_to_all | solution.py:103
  251.9 0.7 add_convert_fusion
  252.6 22.1 %reduce-scatter.2.cloned.1.call-done = bf16[256,512]{0,1:T(8,128)(2,1)} async-done(((bf16[2048,512]{0,1:T(8,128)(2,1)}), bf16[256,512]{0,1:T(8,128)(2,1)}) %reduce-scatter.2.cloned.1.call-update) | async-done | bytes 262160 | tf_op jit(solution)/shard_map/reduce_scatter | solution.py:117
  274.7 1.9 copy.79
  (74 shorter events, 8.2 us)
Async XLA Ops:
  7.2 183.4 %all-gather.2.cloned.1.call-start = ((), (), s32[]{:S(2)}) async-start(), calls=%async_computation.4 | async-start | bytes 1310720 | tf_op jit(solution)/shard_map/all_gather | solution.py:20
  7.9 266.8 %reduce-scatter.2.cloned.1.call-start = ((), (), s32[]{:S(2)}) async-start(), calls=%async_computation.5 | async-start | bytes 2359296 | tf_op jit(solution)/shard_map/reduce_scatter | solution.py:117
  92.5 1.9 copy-start
  111.8 3.6 %copy-start.1 = (f32[2,1024,128,4]{2,1,3,0:T(8,128)S(1)}, f32[2,1024,128,4]{2,1,3,0:T(8,128)}, u32[]{:S(2)}) copy-start(f32[2,1024,128,4]{2,1,3,0:T(8,128)} %copy-done) | copy-start | bytes 12582916 | tf_op jit(solution)/shard_map/while
  111.8 3.6 %copy-start.4 = (bf16[1024,128]{0,1:T(8,128)(2,1)S(1)}, bf16[1024,128]{0,1:T(8,128)(2,1)}, u32[]{:S(2)}) copy-start(bf16[1024,128]{0,1:T(8,128)(2,1)} %copy.115) | copy-start | bytes 786436 | tf_op jit(solution)/shard_map/while
  111.9 3.6 %copy-start.5 = (bf16[128,512]{0,1:T(8,128)(2,1)S(1)}, bf16[128,512]{0,1:T(8,128)(2,1)}, u32[]{:S(2)}) copy-start(bf16[128,512]{0,1:T(8,128)(2,1)} %copy.116) | copy-start | bytes 393220 | tf_op jit(solution)/shard_map/while
  115.5 2.8 copy-start.3
  116.9 1.4 copy-start.2
  150.5 1.9 copy-start
  169.9 3.6 %copy-start.1 = (f32[2,1024,128,4]{2,1,3,0:T(8,128)S(1)}, f32[2,1024,128,4]{2,1,3,0:T(8,128)}, u32[]{:S(2)}) copy-start(f32[2,1024,128,4]{2,1,3,0:T(8,128)} %copy-done) | copy-start | bytes 12582916 | tf_op jit(solution)/shard_map/while
  169.9 3.6 %copy-start.4 = (bf16[1024,128]{0,1:T(8,128)(2,1)S(1)}, bf16[1024,128]{0,1:T(8,128)(2,1)}, u32[]{:S(2)}) copy-start(bf16[1024,128]{0,1:T(8,128)(2,1)} %copy.115) | copy-start | bytes 786436 | tf_op jit(solution)/shard_map/while
  169.9 3.6 %copy-start.5 = (bf16[128,512]{0,1:T(8,128)(2,1)S(1)}, bf16[128,512]{0,1:T(8,128)(2,1)}, u32[]{:S(2)}) copy-start(bf16[128,512]{0,1:T(8,128)(2,1)} %copy.116) | copy-start | bytes 393220 | tf_op jit(solution)/shard_map/while
  173.5 2.8 copy-start.3
  174.9 1.4 copy-start.2
  190.5 13.9 %copy-start.6 = (bf16[2,128,512]{2,1,0:T(8,128)(2,1)}, bf16[2,128,512]{2,1,0:T(8,128)(2,1)S(1)}, u32[]{:S(2)}) copy-start(bf16[2,128,512]{2,1,0:T(8,128)(2,1)S(1)} %copy.72) | copy-start | bytes 786436
  196.4 12.3 %all-to-all-start = ((s32[8,1,2]{2,1,0:T(1,128)}), s32[8,1,2]{2,1,0:T(1,128)S(1)}, u32[]{:S(2)}, u32[]{:S(2)}) async-start(s32[8,1,2]{2,1,0:T(1,128)} %copy.74), calls=%async_computation | async-start | bytes 8192 | tf_op jit(solution)/shard_map/all_to_all | solution.py:104
  235.6 15.6 %all-to-all-start.2 = ((f32[8,2,64,128]{3,2,1,0:T(8,128)}), f32[8,2,64,128]{3,2,1,0:T(8,128)S(1)}, u32[]{:S(2)}, u32[]{:S(2)}) async-start(f32[8,2,64,128]{3,2,1,0:T(8,128)} %get-tuple-element.189), calls=%async_computation.2 | async-start | bytes 1048576 | tf_op jit(solution)/shard_map/all_to_all | solution.py:103
Sparse Core Ops, SparseCore 0:
  9.5 19.4 all-gather.1
  194.1 80.5 reduce-scatter.1
where the time goes:
time: 285 us; the launch traced here: 283 us
  blocking collectives  91.5 us (32%)
  local copies, waits for them, and re-layouts  58.3 us (20%)
  other arithmetic  39.1 us (14%)
  waiting for transfers between devices  33.2 us (12%)
  matrix products  33.2 us (12%)
  between operations  14.1 us (5%)
  starting transfers between devices  11.2 us (4%)
    all_gather x1, blocking collectives, body(): lax.all_gather(value_rows_by_head, 'kv', axis=0, tiled=True)  33.3 us
    all_gather x1, blocking collectives, body(): lax.all_gather(key_vectors, 'kv', axis=0, tiled=True)  31.4 us
    all_to_all x1, blocking collectives, body(): lax.all_to_all(send_k, 'kv', split_axis=0, concat_axis=0, tiled=True)  26.8 us
    reduce_scatter x1, waiting for transfers between devices, body(): lax.psum_scatter(jnp.einsum('tr,tc->rc', whole_inputs, query_grad, prefer...  22.1 us
    scatter-add x2, other arithmetic, summed_step(): acc_v.at[key_rows].add(d_value)  13.6 us
    scatter-add x2, other arithmetic, summed_step(): acc_k.at[key_rows].add(d_key)  13.6 us
    gather x2, local copies, waits for them, and re-layouts, attend_block(): jnp.take(all_keys, key_rows, axis=0).reshape(-1, kv_heads, HEAD_SIZE)  8.62 us
    dot_general x2, matrix products, attend_block(): jnp.einsum('kgts,tkgd->skd', probs_half, g_block, preferred_element_type=...  8.29 us
  transfers between devices with their start and end apart: 4, of which 3 were waited for; matrix products, arithmetic and copies ran while one was open for 42% of the time, Pallas kernels for 0%

commit v1 on v0

v1 whole, which is shorter than its diff:
```python
import functools

import jax
import jax.numpy as jnp
from jax import lax
from jax.experimental import pallas as pl
from jax.experimental.pallas import tpu as pltpu
from jax.sharding import PartitionSpec as P

HEAD_SIZE = 64
QB = 128
KB = 64
HEADS_PER_KEY = 4
NEG = -1e30
BF16 = jnp.bfloat16
F32 = jnp.float32


def dot_nt(x, y):
    return lax.dot_general(x, y, (((1,), (1,)), ((), ())), preferred_element_type=F32)


def dot_nn(x, y):
    return lax.dot_general(x, y, (((1,), (0,)), ((), ())), preferred_element_type=F32)


def dot_tn(x, y):
    return lax.dot_general(x, y, (((0,), (0,)), ((), ())), preferred_element_type=F32)


def kernel(
    n, tp, a, b,
    sel_ref, x_ref, q_ref, k_ref, v_ref, g_ref,
    dq_ref, dk_ref, dv_ref, w_ref,
    kvst, kvbuf, xst, xbuf, q_s, g_s, s_buf, dp_buf, dq_acc, gst, grecv, own_acc,
    qall, wst, wrecv, w_own,
    kv_send, kv_recv, x_send, x_recv, g_send, g_recv, q_send, q_recv, w_send, w_recv,
):
    me = lax.axis_index("kv")
    t = lax.axis_index("tp")
    alpha = lax.rem(me, a)
    beta = lax.div(me, a)
    rows, cols = k_ref.shape
    heads = cols // HEAD_SIZE
    group = q_ref.shape[1] // cols
    local = rows // QB
    owner = rows // KB
    chunk = local * KB
    own_chunks = rows // chunk
    wide = group * rows
    width = xst.shape[2]
    n_chunk = xst.shape[0]
    gcols = group * HEAD_SIZE
    scale = HEAD_SIZE ** (-0.5)

    def remote(src, dst, send, recv, kv, tpi):
        return pltpu.make_async_remote_copy(
            src_ref=src, dst_ref=dst, send_sem=send, recv_sem=recv,
            device_id=(kv, tpi), device_id_type=pl.DeviceIdType.MESH,
        )

    barrier = pltpu.get_barrier_semaphore()
    for d in range(1, n):
        pl.semaphore_signal(
            barrier, inc=1, device_id=(lax.rem(me + d, n), t), device_id_type=pl.DeviceIdType.MESH
        )
    for d in range(1, tp):
        for m in range(a):
            pl.semaphore_signal(
                barrier, inc=1, device_id=(beta * a + m, lax.rem(t + d, tp)),
                device_id_type=pl.DeviceIdType.MESH,
            )

    def slots(i, j):
        used = []
        for blk in range(owner):
            u = sel_ref[i * local, j * owner + blk]
            for r in range(1, local):
                u = jnp.maximum(u, sel_ref[i * local + r, j * owner + blk])
            used.append(u)
        picks = []
        for p in range(local):
            before = jnp.int32(0)
            one = []
            for blk in range(owner):
                one.append(jnp.where(before == p, used[blk], 0))
                before = before + used[blk]
            picks.append(one)
        return picks

    def stage_kv(i, carry):
        picks = slots(i, me)
        for p in range(local):
            at = slice(p * KB, (p + 1) * KB)
            for ref, first in ((k_ref, 0), (v_ref, cols)):
                out = jnp.zeros((KB, cols), F32)
                for blk in range(owner):
                    rows_of = ref[blk * KB : (blk + 1) * KB, :].astype(F32)
                    out = jnp.where(picks[p][blk] > 0, rows_of, out)
                kvst[i, at, first : first + cols] = out.astype(BF16)
        return carry

    lax.fori_loop(me + 1, n, stage_kv, 0)
    for q in range(n_chunk):
        xst[q] = x_ref[:, q * width : (q + 1) * width]

    pl.semaphore_wait(barrier, n - 1 + (tp - 1) * a)

    def kv_copy(i, j):
        return remote(kvst.at[i], kvbuf.at[j], kv_send.at[i], kv_recv.at[j], i, t)

    def start_kv(i, carry):
        kv_copy(i, me).start()
        return carry

    lax.fori_loop(me + 1, n, start_kv, 0)

    def x_copy(q, tt):
        c = t * n_chunk + q
        return remote(
            xst.at[q], xbuf.at[alpha, lax.div(c, a)], x_send.at[q, tt],
            x_recv.at[alpha, lax.div(c, a)], beta * a + lax.rem(c, a), tt,
        )

    for q in range(n_chunk):
        c = t * n_chunk + q
        for tt in range(tp):
            mine = jnp.logical_and(lax.rem(c, a) == alpha, t == tt)

            @pl.when(jnp.logical_not(mine))
            def _():
                x_copy(q, tt).start()

            @pl.when(mine)
            def _():
                xbuf[alpha, lax.div(c, a)] = x_ref[:, q * width : (q + 1) * width]

    lane = lax.rem(lax.broadcasted_iota(jnp.int32, (1, wide), 1), rows)
    lane_block = lax.div(lane, QB)

    def row_bias(flags):
        vals = [jnp.where(f > 0, F32(0.0), F32(NEG)) for f in flags]
        out = jnp.full((1, wide), vals[0], F32)
        for r in range(1, local):
            out = jnp.where(lane_block == r, vals[r], out)
        return out

    def head_cols(h):
        return slice(h * HEAD_SIZE, (h + 1) * HEAD_SIZE)

    def own_kv(o, h):
        at = slice(o * chunk, (o + 1) * chunk)
        return k_ref[at, head_cols(h)], v_ref[at, head_cols(h)]

    def far_k(j, h):
        return kvbuf[j, :, head_cols(h)]

    def far_v(j, h):
        return kvbuf[j, :, cols + h * HEAD_SIZE : cols + (h + 1) * HEAD_SIZE]

    def g_copy(h, i, j):
        return remote(gst.at[h, j], grecv.at[h, i], g_send.at[h, j], g_recv.at[h, i], j, t)

    def q_copy(h, m):
        return remote(
            qall.at[h, alpha], qall.at[h, alpha], q_send.at[h, m], q_recv.at[h, alpha],
            beta * a + m, t,
        )

    def w_copy(h, bb):
        return remote(
            wst.at[h, bb], wrecv.at[h, beta], w_send.at[h, bb], w_recv.at[h, beta],
            bb * a + alpha, t,
        )

    def score_own(o, h):
        k, _ = own_kv(o, h)
        s = dot_nt(k, q_s[...])
        parts = []
        for p in range(local):
            blk = o * local + p
            bias = row_bias([sel_ref[me * local + r, me * owner + blk] for r in range(local)])
            key = blk * KB + lax.broadcasted_iota(jnp.int32, (KB, wide), 0)
            parts.append(jnp.where(key <= lane, s[p * KB : (p + 1) * KB] + bias, NEG))
        return jnp.concatenate(parts, axis=0)

    def attend(h, wait_kv):
        for gr in range(group):
            hh = h * group + gr
            at = slice(gr * rows, (gr + 1) * rows)
            q_s[at, :] = (q_ref[:, head_cols(hh)].astype(F32) * scale).astype(BF16)
            g_s[at, :] = g_ref[:, head_cols(hh)]
        m = jnp.full((1, wide), NEG, F32)
        for o in range(own_chunks):
            s = score_own(o, h)
            s_buf[o] = s
            m = jnp.maximum(m, jnp.max(s, axis=0, keepdims=True))

        def pass_a(j, m):
            if wait_kv:
                kv_copy(j, j).wait_recv()
            picks = slots(me, j)
            s = dot_nt(far_k(j, h), q_s[...])
            parts = []
            for p in range(local):
                flags = []
                for r in range(local):
                    f = jnp.int32(0)
                    for blk in range(owner):
                        f = f + picks[p][blk] * sel_ref[me * local + r, j * owner + blk]
                    flags.append(f)
                parts.append(s[p * KB : (p + 1) * KB] + row_bias(flags))
            s = jnp.concatenate(parts, axis=0)
            s_buf[own_chunks + j] = s
            return jnp.maximum(m, jnp.max(s, axis=0, keepdims=True))

        m = lax.fori_loop(0, me, pass_a, m)

        def pass_b(idx, v, l, rd):
            p = jnp.exp(s_buf[idx] - m)
            dp = dot_nt(v, g_s[...])
            s_buf[idx] = p
            dp_buf[idx] = dp
            return (
                l + jnp.sum(p, axis=0, keepdims=True),
                rd + jnp.sum(p * dp, axis=0, keepdims=True),
            )

        l = jnp.zeros((1, wide), F32)
        rd = jnp.zeros((1, wide), F32)
        for o in range(own_chunks):
            l, rd = pass_b(o, own_kv(o, h)[1], l, rd)
        l, rd = lax.fori_loop(
            0, me, lambda j, c: pass_b(own_chunks + j, far_v(j, h), c[0], c[1]), (l, rd)
        )
        inv = 1.0 / l
        rd = rd * inv

        def pass_c(idx, k):
            pn = s_buf[idx] * inv
            ds = (pn * (dp_buf[idx] - rd)).astype(BF16)
            dv = dot_nn(pn.astype(BF16), g_s[...])
            dk = dot_nn(ds, q_s[...])
            return dot_tn(ds, k), dk, dv

        def far_c(j, carry):
            dq, dk, dv = pass_c(own_chunks + j, far_k(j, h))
            gst[h, j, :, 0:HEAD_SIZE] = dk.astype(BF16)
            gst[h, j, :, HEAD_SIZE : 2 * HEAD_SIZE] = dv.astype(BF16)
            dq_acc[...] += dq
            g_copy(h, me, j).start()
            return carry

        for o in range(own_chunks):
            dq, dk, dv = pass_c(o, own_kv(o, h)[0])
            at = slice(o * chunk, (o + 1) * chunk)
            own_acc[h, at, 0:HEAD_SIZE] = dk
            own_acc[h, at, HEAD_SIZE : 2 * HEAD_SIZE] = dv
            if o == 0:
                dq_acc[...] = dq
            else:
                dq_acc[...] += dq
        lax.fori_loop(0, me, far_c, 0)
        for gr in range(group):
            part = (dq_acc[gr * rows : (gr + 1) * rows, :] * scale).astype(BF16)
            dq_ref[:, head_cols(h * group + gr)] = part
            qall[h, alpha, :, head_cols(gr)] = part
        for mm in range(a):

            @pl.when(alpha != mm)
            def _():
                q_copy(h, mm).start()

    def weight_part(h, wait_x):
        if wait_x:
            for m in range(a):
                for bb in range(b):
                    own = jnp.logical_and(alpha == m, lax.div(bb * a + alpha, n_chunk) == t)

                    @pl.when(jnp.logical_not(own))
                    def _():
                        remote(
                            xst.at[0], xbuf.at[m, bb], x_send.at[0, 0], x_recv.at[m, bb], me, t
                        ).wait_recv()

        for mm in range(a):

            @pl.when(alpha != mm)
            def _():
                remote(
                    qall.at[h, mm], qall.at[h, mm], q_send.at[h, mm], q_recv.at[h, mm], me, t
                ).wait_recv()

        def partial(bb):
            out = dot_tn(xbuf[0, bb], qall[h, 0])
            for m in range(1, a):
                out = out + dot_tn(xbuf[m, bb], qall[h, m])
            return out

        for d in range(1, b):
            bb = lax.rem(beta + d, b)
            wst[h, bb] = partial(bb).astype(BF16)
            w_copy(h, bb).start()
        w_own[h] = partial(beta)

    for h in range(heads):
        attend(h, h == 0)
    for h in range(heads):
        weight_part(h, h == 0)

    for h in range(heads):

        def add_far(i, carry):
            remote(gst.at[h, 0], grecv.at[h, i], g_send.at[h, 0], g_recv.at[h, i], me, t).wait_recv()
            picks = slots(i, me)
            for p in range(local):
                got = grecv[h, i, p * KB : (p + 1) * KB, :].astype(F32)
                for blk in range(owner):
                    own_acc[h, blk * KB : (blk + 1) * KB, :] += jnp.where(
                        picks[p][blk] > 0, got, 0.0
                    )
            return carry

        lax.fori_loop(me + 1, n, add_far, 0)
        dk_ref[:, head_cols(h)] = own_acc[h, :, 0:HEAD_SIZE].astype(BF16)
        dv_ref[:, head_cols(h)] = own_acc[h, :, HEAD_SIZE : 2 * HEAD_SIZE].astype(BF16)

    for h in range(heads):
        total = w_own[h]
        for d in range(1, b):
            bb = lax.rem(beta + d, b)
            remote(
                wst.at[h, bb], wrecv.at[h, bb], w_send.at[h, bb], w_recv.at[h, bb], me, t
            ).wait_recv()
            total = total + wrecv[h, bb].astype(F32)
        w_ref[:, h * gcols : (h + 1) * gcols] = total

    def done_kv(i, carry):
        kv_copy(i, me).wait_send()
        return carry

    lax.fori_loop(me + 1, n, done_kv, 0)
    for q in range(n_chunk):
        c = t * n_chunk + q
        for tt in range(tp):

            @pl.when(jnp.logical_not(jnp.logical_and(lax.rem(c, a) == alpha, t == tt)))
            def _():
                x_copy(q, tt).wait_send()

    for h in range(heads):

        def done_g(j, carry):
            g_copy(h, me, j).wait_send()
            return carry

        lax.fori_loop(0, me, done_g, 0)
        for mm in range(a):

            @pl.when(alpha != mm)
            def _():
                q_copy(h, mm).wait_send()

        for d in range(1, b):
            w_copy(h, lax.rem(beta + d, b)).wait_send()


def body(n, tp, inputs, queries, key_vectors, value_rows_by_head, out_grad, chosen):
    rows, cols = key_vectors.shape
    q_cols = queries.shape[1]
    heads = cols // HEAD_SIZE
    group = q_cols // cols
    local = rows // QB
    chunk = local * KB
    own_chunks = rows // chunk
    wide = group * rows
    d_model = inputs.shape[1] * tp
    width = d_model // n
    n_chunk = inputs.shape[1] // width
    a = 4
    b = n // a
    gcols = group * HEAD_SIZE
    blocks = n * rows // KB
    sel = jnp.any(
        chosen[:, :, None] == jnp.arange(blocks, dtype=jnp.int32)[None, None, :], axis=1
    ).astype(jnp.int32)
    vmem = pl.BlockSpec(memory_space=pltpu.VMEM)
    dma = pltpu.SemaphoreType.DMA
    return pl.pallas_call(
        functools.partial(kernel, n, tp, a, b),
        out_shape=(
            jax.ShapeDtypeStruct((rows, q_cols), BF16),
            jax.ShapeDtypeStruct((rows, cols), BF16),
            jax.ShapeDtypeStruct((rows, cols), BF16),
            jax.ShapeDtypeStruct((width, q_cols), F32),
        ),
        in_specs=[pl.BlockSpec(memory_space=pltpu.SMEM)] + [vmem] * 5,
        out_specs=(vmem,) * 4,
        scratch_shapes=[
            pltpu.VMEM((n, chunk, 2 * cols), BF16),
            pltpu.VMEM((n, chunk, 2 * cols), BF16),
            pltpu.VMEM((n_chunk, rows, width), BF16),
            pltpu.VMEM((a, b, rows, width), BF16),
            pltpu.VMEM((wide, HEAD_SIZE), BF16),
            pltpu.VMEM((wide, HEAD_SIZE), BF16),
            pltpu.VMEM((own_chunks + n - 1, chunk, wide), F32),
            pltpu.VMEM((own_chunks + n - 1, chunk, wide), F32),
            pltpu.VMEM((wide, HEAD_SIZE), F32),
            pltpu.VMEM((heads, n, chunk, 2 * HEAD_SIZE), BF16),
            pltpu.VMEM((heads, n, chunk, 2 * HEAD_SIZE), BF16),
            pltpu.VMEM((heads, rows, 2 * HEAD_SIZE), F32),
            pltpu.VMEM((heads, a, rows, gcols), BF16),
            pltpu.VMEM((heads, b, width, gcols), BF16),
            pltpu.VMEM((heads, b, width, gcols), BF16),
            pltpu.VMEM((heads, width, gcols), F32),
            dma((n,)),
            dma((n,)),
            dma((n_chunk, tp)),
            dma((a, b)),
            dma((heads, n)),
            dma((heads, n)),
            dma((heads, a)),
            dma((heads, a)),
            dma((heads, b)),
            dma((heads, b)),
        ],
        compiler_params=pltpu.CompilerParams(
            collective_id=0, has_side_effects=True, vmem_limit_bytes=60 * 1024 * 1024
        ),
    )(sel, inputs, queries, key_vectors, value_rows_by_head, out_grad)


def solution(mesh):
    n, tp = mesh.shape["kv"], mesh.shape["tp"]
    placed = (P("kv", "tp"),) * 5 + (P(),)
    return jax.shard_map(
        functools.partial(body, n, tp),
        mesh=mesh,
        in_specs=placed,
        out_specs=(P("kv", "tp"),) * 4,
        check_vma=False,
    )
```

time: 285 us -> 60.8 us (0.21)
  the two profiles are of different devices: /device:TPU:0 before, /device:TPU:3 now
where the time goes in v1:
time: 60.8 us; the launch traced here: 60.5 us
  Pallas kernels  53.8 us (88%)
  local copies, waits for them, and re-layouts  4.66 us (8%)
  other arithmetic  1.42 us (2%)
  between operations  0.65 us (1%)
    pallas_call x1, Pallas kernels, body(): pl.pallas_call(functools.partial(kernel, n, tp, a, b), out_shape=(jax.Sha...  53.8 us
    unnamed x8, local copies, waits for them, and re-layouts  4.66 us

profile of v1, /device:TPU:3, one launch (start us, length us, event | category | flops | bytes accessed | tf_op | source)
XLA Modules:
  0.0 60.5 jit_solution(156491135015090388)
XLA Ops:
  0.6 0.8 %fusion = pred[16,32]{1,0:T(8,128)(4,1)S(1)} fusion(s32[16,16]{1,0:T(8,128)} %param.11), kind=kLoop, calls=%fused_computation.1 | loop fusion | flops 15872 | bytes 1536 | tf_op jit(solution)/shard_map/reduce_or | solution.py:384
  1.4 0.6 %convert_element_type.3.sel_ref = s32[16,32]{1,0:T(8,128)} convert(pred[16,32]{1,0:T(8,128)(4,1)S(1)} %fusion) | non-fusion elementwise | flops 512 | bytes 2560 | tf_op jit(solution)/shard_map/convert_element_type | solution.py:386
  2.1 53.8 %shard_map.93 = (bf16[256,512]{1,0:T(8,128)(2,1)}, bf16[256,128]{1,0:T(8,128)(2,1)}, bf16[256,128]{1,0:T(8,128)(2,1)}, f32[256,512]{1,0:T(8,128)}) custom-call(s32[16,32]{1,0:T(8,128)} %convert_element_type.3.sel_ref, bf16[256,512]{1,0:T(8,128)(2,1)} %x_ref.1, bf16[256,512]{1,0:T(8,128)(2,1)} %q_ref.1, bf16[256,128]{1,0:T(8,128)(2,1)} %k_ref.1, ...), custom_call_target="tpu_custom_call" | custom-call | tf_op jit(solution)/shard_map/pallas_call | solution.py:389
  55.9 0.0 copy-start
  55.9 1.7 %copy.14 = bf16[256,512]{1,0:T(8,128)(2,1)} copy(bf16[256,512]{1,0:T(8,128)(2,1)} %get-tuple-element.8) | data formatting | bytes 524288
  57.6 0.0 copy-start.1
  57.6 1.5 %copy.15 = bf16[256,128]{1,0:T(8,128)(2,1)} copy(bf16[256,128]{1,0:T(8,128)(2,1)} %get-tuple-element.9) | data formatting | bytes 131072
  59.1 0.0 copy-done.1
  59.1 0.6 %copy.16 = bf16[256,128]{1,0:T(8,128)(2,1)} copy(bf16[256,128]{1,0:T(8,128)(2,1)S(1)} %copy-done.1) | data formatting | bytes 131072
  59.7 0.0 copy-done
  59.7 0.8 %copy.17 = f32[256,512]{1,0:T(8,128)} copy(f32[256,512]{1,0:T(8,128)S(1)} %copy-done) | data formatting | bytes 1048576
Async XLA Ops:
  55.9 3.9 %copy-start = (f32[256,512]{1,0:T(8,128)S(1)}, f32[256,512]{1,0:T(8,128)}, u32[]{:S(2)}) copy-start(f32[256,512]{1,0:T(8,128)} %get-tuple-element.11) | copy-start | bytes 1572868
  57.6 1.5 %copy-start.1 = (bf16[256,128]{1,0:T(8,128)(2,1)S(1)}, bf16[256,128]{1,0:T(8,128)(2,1)}, u32[]{:S(2)}) copy-start(bf16[256,128]{1,0:T(8,128)(2,1)} %get-tuple-element.10) | copy-start | bytes 196612

commit v2 on v1

--- a/solution.py
+++ b/solution.py
@@ -10,6 +10,7 @@
 HEAD_SIZE = 64
 QB = 128
 KB = 64
+PARTS = 2
 HEADS_PER_KEY = 4
 NEG = -1e30
 BF16 = jnp.bfloat16
@@ -32,9 +33,9 @@
     n, tp, a, b,
     sel_ref, x_ref, q_ref, k_ref, v_ref, g_ref,
     dq_ref, dk_ref, dv_ref, w_ref,
-    kvst, kvbuf, xst, xbuf, q_s, g_s, s_buf, dp_buf, dq_acc, gst, grecv, own_acc,
+    kvst, kvbuf, xst, xbuf, q_s, g_s, s_buf, dp_buf, dq_acc, far_acc, gst, grecv, own_acc,
     qall, wst, wrecv, w_own,
-    kv_send, kv_recv, x_send, x_recv, g_send, g_recv, q_send, q_recv, w_send, w_recv,
+    kv_send, kv_recv, x_send, xf_send, x_recv, g_send, g_recv, q_send, q_recv, w_send, w_recv,
 ):
     me = lax.axis_index("kv")
     t = lax.axis_index("tp")
@@ -47,10 +48,11 @@
     owner = rows // KB
     chunk = local * KB
     own_chunks = rows // chunk
-    wide = group * rows
+    sub = group // PARTS
+    wide = sub * rows
     width = xst.shape[2]
     n_chunk = xst.shape[0]
-    gcols = group * HEAD_SIZE
+    gcols = sub * HEAD_SIZE
     scale = HEAD_SIZE ** (-0.5)
 
     def remote(src, dst, send, recv, kv, tpi):
@@ -115,25 +117,45 @@
 
     lax.fori_loop(me + 1, n, start_kv, 0)
 
-    def x_copy(q, tt):
+    def x_copy(q):
         c = t * n_chunk + q
         return remote(
-            xst.at[q], xbuf.at[alpha, lax.div(c, a)], x_send.at[q, tt],
-            x_recv.at[alpha, lax.div(c, a)], beta * a + lax.rem(c, a), tt,
+            xst.at[q], xbuf.at[alpha, lax.div(c, a)], x_send.at[q],
+            x_recv.at[alpha, lax.div(c, a)], beta * a + lax.rem(c, a), t,
         )
 
     for q in range(n_chunk):
         c = t * n_chunk + q
-        for tt in range(tp):
-            mine = jnp.logical_and(lax.rem(c, a) == alpha, t == tt)
-
-            @pl.when(jnp.logical_not(mine))
+        mine = lax.rem(c, a) == alpha
+
+        @pl.when(jnp.logical_not(mine))
+        def _():
+            x_copy(q).start()
+
+        @pl.when(mine)
+        def _():
+            xbuf[alpha, lax.div(c, a)] = x_ref[:, q * width : (q + 1) * width]
+
+    def x_hand(q, m, d):
+        slot = xbuf.at[m, lax.div(t * n_chunk + q, a)]
+        return remote(
+            slot, slot, xf_send.at[q, m, d - 1], x_recv.at[m, lax.div(t * n_chunk + q, a)],
+            me, lax.rem(t + d, tp),
+        )
+
+    def forward_x():
+        for q in range(n_chunk):
+
+            @pl.when(lax.rem(t * n_chunk + q, a) == alpha)
             def _():
-                x_copy(q, tt).start()
-
-            @pl.when(mine)
-            def _():
-                xbuf[alpha, lax.div(c, a)] = x_ref[:, q * width : (q + 1) * width]
+                for m in range(a):
+
+                    @pl.when(alpha != m)
+                    def _():
+                        x_hand(q, m, 1).wait_recv()
+
+                    for d in range(1, tp):
+                        x_hand(q, m, d).start()
 
     lane = lax.rem(lax.broadcasted_iota(jnp.int32, (1, wide), 1), rows)
     lane_block = lax.div(lane, QB)
@@ -184,9 +206,10 @@
             parts.append(jnp.where(key <= lane, s[p * KB : (p + 1) * KB] + bias, NEG))
         return jnp.concatenate(parts, axis=0)
 
-    def attend(h, wait_kv):
-        for gr in range(group):
-            hh = h * group + gr
+    def attend(u, wait_kv):
+        h, part = u // PARTS, u % PARTS
+        for gr in range(sub):
+            hh = u * sub + gr
             at = slice(gr * rows, (gr + 1) * rows)
             q_s[at, :] = (q_ref[:, head_cols(hh)].astype(F32) * scale).astype(BF16)
             g_s[at, :] = g_ref[:, head_cols(hh)]
@@ -215,6 +238,8 @@
             return jnp.maximum(m, jnp.max(s, axis=0, keepdims=True))
 
         m = lax.fori_loop(0, me, pass_a, m)
+        if wait_kv:
+            forward_x()
 
         def pass_b(idx, v, l, rd):
             p = jnp.exp(s_buf[idx] - m)
@@ -233,6 +258,8 @@
         l, rd = lax.fori_loop(
             0, me, lambda j, c: pass_b(own_chunks + j, far_v(j, h), c[0], c[1]), (l, rd)
         )
+        if u > 0:
+            weight_part(u - 1, u == 1)
         inv = 1.0 / l
         rd = rd * inv
 
@@ -245,42 +272,51 @@
 
         def far_c(j, carry):
             dq, dk, dv = pass_c(own_chunks + j, far_k(j, h))
-            gst[h, j, :, 0:HEAD_SIZE] = dk.astype(BF16)
-            gst[h, j, :, HEAD_SIZE : 2 * HEAD_SIZE] = dv.astype(BF16)
+            both = jnp.concatenate([dk, dv], axis=1)
+            if part > 0:
+                both = both + far_acc[j]
+            if part < PARTS - 1:
+                far_acc[j] = both
+            else:
+                gst[h, j] = both.astype(BF16)
             dq_acc[...] += dq
-            g_copy(h, me, j).start()
             return carry
 
         for o in range(own_chunks):
             dq, dk, dv = pass_c(o, own_kv(o, h)[0])
             at = slice(o * chunk, (o + 1) * chunk)
-            own_acc[h, at, 0:HEAD_SIZE] = dk
-            own_acc[h, at, HEAD_SIZE : 2 * HEAD_SIZE] = dv
+            both = jnp.concatenate([dk, dv], axis=1)
+            own_acc[h, at, :] = both if part == 0 else own_acc[h, at, :] + both
             if o == 0:
                 dq_acc[...] = dq
             else:
                 dq_acc[...] += dq
         lax.fori_loop(0, me, far_c, 0)
-        for gr in range(group):
-            part = (dq_acc[gr * rows : (gr + 1) * rows, :] * scale).astype(BF16)
-            dq_ref[:, head_cols(h * group + gr)] = part
-            qall[h, alpha, :, head_cols(gr)] = part
+        for gr in range(sub):
+            done = (dq_acc[gr * rows : (gr + 1) * rows, :] * scale).astype(BF16)
+            dq_ref[:, head_cols(u * sub + gr)] = done
+            qall[u, alpha, :, head_cols(gr)] = done
         for mm in range(a):
 
             @pl.when(alpha != mm)
             def _():
-                q_copy(h, mm).start()
+                q_copy(u, mm).start()
+
+        def send_g(j, carry):
+            g_copy(h, me, j).start()
+            return carry
+
+        if part == PARTS - 1:
+            lax.fori_loop(0, me, send_g, 0)
 
     def weight_part(h, wait_x):
         if wait_x:
             for m in range(a):
                 for bb in range(b):
-                    own = jnp.logical_and(alpha == m, lax.div(bb * a + alpha, n_chunk) == t)
-
-                    @pl.when(jnp.logical_not(own))
+                    @pl.when(lax.div(bb * a + alpha, n_chunk) != t)
                     def _():
                         remote(
-                            xst.at[0], xbuf.at[m, bb], x_send.at[0, 0], x_recv.at[m, bb], me, t
+                            xst.at[0], xbuf.at[m, bb], x_send.at[0], x_recv.at[m, bb], me, t
                         ).wait_recv()
 
         for mm in range(a):
@@ -303,10 +339,10 @@
             w_copy(h, bb).start()
         w_own[h] = partial(beta)
 
-    for h in range(heads):
-        attend(h, h == 0)
-    for h in range(heads):
-        weight_part(h, h == 0)
+    units = heads * PARTS
+    for u in range(units):
+        attend(u, u == 0)
+    weight_part(units - 1, units == 1)
 
     for h in range(heads):
 
@@ -325,7 +361,7 @@
         dk_ref[:, head_cols(h)] = own_acc[h, :, 0:HEAD_SIZE].astype(BF16)
         dv_ref[:, head_cols(h)] = own_acc[h, :, HEAD_SIZE : 2 * HEAD_SIZE].astype(BF16)
 
-    for h in range(heads):
+    for h in range(units):
         total = w_own[h]
         for d in range(1, b):
             bb = lax.rem(beta + d, b)
@@ -341,12 +377,17 @@
 
     lax.fori_loop(me + 1, n, done_kv, 0)
     for q in range(n_chunk):
-        c = t * n_chunk + q
-        for tt in range(tp):
-
-            @pl.when(jnp.logical_not(jnp.logical_and(lax.rem(c, a) == alpha, t == tt)))
-            def _():
-                x_copy(q, tt).wait_send()
+        mine = lax.rem(t * n_chunk + q, a) == alpha
+
+        @pl.when(jnp.logical_not(mine))
+        def _():
+            x_copy(q).wait_send()
+
+        @pl.when(mine)
+        def _():
+            for m in range(a):
+                for d in range(1, tp):
+                    x_hand(q, m, d).wait_send()
 
     for h in range(heads):
 
@@ -355,6 +396,7 @@
             return carry
 
         lax.fori_loop(0, me, done_g, 0)
+    for h in range(units):
         for mm in range(a):
 
             @pl.when(alpha != mm)
@@ -363,6 +405,11 @@
 
         for d in range(1, b):
             w_copy(h, lax.rem(beta + d, b)).wait_send()
+
+
+def hand_out(*refs):
+    for src, dst in zip(refs[:4], refs[4:]):
+        dst[...] = src[...]
 
 
 def body(n, tp, inputs, queries, key_vectors, value_rows_by_head, out_grad, chosen):
@@ -373,27 +420,28 @@
     local = rows // QB
     chunk = local * KB
     own_chunks = rows // chunk
-    wide = group * rows
+    sub = group // PARTS
+    wide = sub * rows
     d_model = inputs.shape[1] * tp
     width = d_model // n
     n_chunk = inputs.shape[1] // width
     a = 4
     b = n // a
-    gcols = group * HEAD_SIZE
+    gcols = sub * HEAD_SIZE
     blocks = n * rows // KB
-    sel = jnp.any(
-        chosen[:, :, None] == jnp.arange(blocks, dtype=jnp.int32)[None, None, :], axis=1
-    ).astype(jnp.int32)
+    named = chosen[:, :, None] == jnp.arange(blocks, dtype=jnp.int32)[None, None, :]
+    sel = jnp.sum(named.astype(jnp.int32), axis=1)
     vmem = pl.BlockSpec(memory_space=pltpu.VMEM)
     dma = pltpu.SemaphoreType.DMA
-    return pl.pallas_call(
+    shapes = (
+        jax.ShapeDtypeStruct((rows, q_cols), BF16),
+        jax.ShapeDtypeStruct((rows, cols), BF16),
+        jax.ShapeDtypeStruct((rows, cols), BF16),
+        jax.ShapeDtypeStruct((width, q_cols), F32),
+    )
+    grads = pl.pallas_call(
         functools.partial(kernel, n, tp, a, b),
-        out_shape=(
-            jax.ShapeDtypeStruct((rows, q_cols), BF16),
-            jax.ShapeDtypeStruct((rows, cols), BF16),
-            jax.ShapeDtypeStruct((rows, cols), BF16),
-            jax.ShapeDtypeStruct((width, q_cols), F32),
-        ),
+        out_shape=shapes,
         in_specs=[pl.BlockSpec(memory_space=pltpu.SMEM)] + [vmem] * 5,
         out_specs=(vmem,) * 4,
         scratch_shapes=[
@@ -406,28 +454,33 @@
             pltpu.VMEM((own_chunks + n - 1, chunk, wide), F32),
             pltpu.VMEM((own_chunks + n - 1, chunk, wide), F32),
             pltpu.VMEM((wide, HEAD_SIZE), F32),
+            pltpu.VMEM((n, chunk, 2 * HEAD_SIZE), F32),
             pltpu.VMEM((heads, n, chunk, 2 * HEAD_SIZE), BF16),
             pltpu.VMEM((heads, n, chunk, 2 * HEAD_SIZE), BF16),
             pltpu.VMEM((heads, rows, 2 * HEAD_SIZE), F32),
-            pltpu.VMEM((heads, a, rows, gcols), BF16),
-            pltpu.VMEM((heads, b, width, gcols), BF16),
-            pltpu.VMEM((heads, b, width, gcols), BF16),
-            pltpu.VMEM((heads, width, gcols), F32),
+            pltpu.VMEM((heads * PARTS, a, rows, gcols), BF16),
+            pltpu.VMEM((heads * PARTS, b, width, gcols), BF16),
+            pltpu.VMEM((heads * PARTS, b, width, gcols), BF16),
+            pltpu.VMEM((heads * PARTS, width, gcols), F32),
             dma((n,)),
             dma((n,)),
-            dma((n_chunk, tp)),
+            dma((n_chunk,)),
+            dma((n_chunk, a, tp - 1)),
             dma((a, b)),
             dma((heads, n)),
             dma((heads, n)),
-            dma((heads, a)),
-            dma((heads, a)),
-            dma((heads, b)),
-            dma((heads, b)),
+            dma((heads * PARTS, a)),
+            dma((heads * PARTS, a)),
+            dma((heads * PARTS, b)),
+            dma((heads * PARTS, b)),
         ],
         compiler_params=pltpu.CompilerParams(
             collective_id=0, has_side_effects=True, vmem_limit_bytes=60 * 1024 * 1024
         ),
     )(sel, inputs, queries, key_vectors, value_rows_by_head, out_grad)
+    return pl.pallas_call(
+        hand_out, out_shape=shapes, in_specs=[vmem] * 4, out_specs=(vmem,) * 4
+    )(*grads)
 
 
 def solution(mesh):

time: 60.8 us -> 68.9 us (1.13)
  the two profiles are of different devices: /device:TPU:3 before, /device:TPU:0 now
where the time goes in v2:
time: 68.9 us; the launch traced here: 68.7 us
  Pallas kernels  66.6 us (97%)
  other arithmetic  1.41 us (2%)
    pallas_call x1, Pallas kernels, body(): pl.pallas_call(functools.partial(kernel, n, tp, a, b), out_shape=shapes,...  64.5 us
    pallas_call x1, Pallas kernels, body(): pl.pallas_call(hand_out, out_shape=shapes, in_specs=[vmem] * 4, out_specs...  2.12 us
    reduce_sum x1, other arithmetic, body(): sel = jnp.sum(named.astype(jnp.int32), axis=1)  1.41 us

profile of v2, /device:TPU:0, one launch (start us, length us, event | category | flops | bytes accessed | tf_op | source)
XLA Modules:
  0.0 68.7 jit_solution(10663690483744402258)
XLA Ops:
  0.6 1.4 %convert_reduce_fusion.sel_ref = s32[16,32]{1,0:T(8,128)} fusion(s32[16,16]{1,0:T(8,128)} %param.11), kind=kLoop, calls=%fused_computation | loop fusion | flops 24064 | bytes 3072 | tf_op jit(solution)/shard_map/reduce_sum | solution.py:433
  2.0 64.5 %shard_map.93 = (bf16[256,512]{1,0:T(8,128)(2,1)}, bf16[256,128]{1,0:T(8,128)(2,1)}, bf16[256,128]{1,0:T(8,128)(2,1)}, f32[256,512]{1,0:T(8,128)}) custom-call(s32[16,32]{1,0:T(8,128)} %convert_reduce_fusion.sel_ref, bf16[256,512]{1,0:T(8,128)(2,1)} %x_ref.1, bf16[256,512]{1,0:T(8,128)(2,1)} %q_ref.1, bf16[256,128]{1,0:T(8,128)(2,1)} %k_ref.1, ...), custom_call_target="tpu_custom_call" | custom-call | tf_op jit(solution)/shard_map/pallas_call | solution.py:442
  66.6 2.1 %shard_map.94 = (bf16[256,512]{1,0:T(8,128)(2,1)}, bf16[256,128]{1,0:T(8,128)(2,1)}, bf16[256,128]{1,0:T(8,128)(2,1)}, f32[256,512]{1,0:T(8,128)}) custom-call(bf16[256,512]{1,0:T(8,128)(2,1)} %get-tuple-element.8.refs_0_, bf16[256,128]{1,0:T(8,128)(2,1)} %get-tuple-element.9.refs_1_, bf16[256,128]{1,0:T(8,128)(2,1)} %get-tuple-element.10.refs_2_, ...), custom_call_target="tpu_custom_call" | custom-call | tf_op jit(solution)/shard_map/pallas_call | solution.py:481
